TPU v7x, 128 devices: a whole 4x4x4 slice. The times are simulated.
128 devices in a mesh: rep: 2 (over x_hi), fs: 16 (over y, x_lo, core), tp: 4 (over z).
Axes of the slice: x: 4 (x_hi: 2, x_lo: 2; x = x_hi * 2 + x_lo), y: 4, z: 4, core: 2. Of those that a mesh axis runs over, the one named last changes fastest.
Arguments:
- tokens: bfloat16 [16384, 2048], P(('rep', 'fs', 'tp')), may hold values from -3 to 3
- mixer_output: bfloat16 [16384, 2048], P(('rep', 'fs', 'tp')), may hold values from -6 to 6
- early_norm: float32 [2048], replicated, may hold values from 0.75 to 1.25
- early_gate: bfloat16 [2048, 5120], P('fs', 'tp'), may hold values from -0.125 to 0.125
- early_value: bfloat16 [2048, 5120], P('fs', 'tp'), may hold values from -0.125 to 0.125
- early_down: bfloat16 [5120, 2048], P('tp', 'fs'), may hold values from -0.078125 to 0.078125
- early_post: float32 [2048], replicated, may hold values from 0.75 to 1.25
- mixer_gain: float32 [2048], replicated, may hold values from 0.75 to 1.25
- later_norm: float32 [2048], replicated, may hold values from 0.75 to 1.25
- later_gate: bfloat16 [2048, 5120], P('fs', 'tp'), may hold values from -0.125 to 0.125
- later_value: bfloat16 [2048, 5120], P('fs', 'tp'), may hold values from -0.125 to 0.125
- later_down: bfloat16 [5120, 2048], P('tp', 'fs'), may hold values from -0.078125 to 0.078125
- later_post: float32 [2048], replicated, may hold values from 0.75 to 1.25
Outputs:
- layer_out: bfloat16 [16384, 2048], P(('rep', 'fs', 'tp'))
All inputs are finite; a program needn't handle non-finite values.
Results may differ from a plain program's by a relative error of at most 0.015.
Values may be sent and summed in bfloat16 or wider, within the bound.
A program may use at most 128 MiB of HBM per device.

v0:
```python
import jax
import jax.numpy as jnp
from jax import lax
from jax.sharding import PartitionSpec as P

epsilon = 1e-06


def over_all(piece, axis, dim, step, start):

    def gathered(part):
        return lax.all_gather(part, axis, axis=dim, tiled=True)

    return step(start, jax.tree.map(gathered, piece), jnp.int32(0))


def own_rows(product, extent, axis):
    everything = product(jnp.int32(0), lax.axis_size(axis) * extent)
    own = lax.psum_scatter(everything.astype(jnp.bfloat16), axis, scatter_dimension=0, tiled=True)
    return own.astype(jnp.float32)


def rms_scale(values, gain):
    values = values.astype(jnp.float32)
    scale = lax.rsqrt(jnp.mean(values * values, axis=-1, keepdims=True) + epsilon)
    return values * scale * gain


def half_branch(normed, gate_piece, value_piece, down_piece):
    all_rows = lax.all_gather(normed, "tp", axis=0, tiled=True)
    empty = jnp.zeros((all_rows.shape[0], gate_piece.shape[1]), jnp.float32)

    def add_rows(totals, pieces, start):
        columns = lax.dynamic_slice_in_dim(all_rows, start, pieces[0].shape[0], 1)
        gate_part = jnp.dot(columns, pieces[0], preferred_element_type=jnp.float32)
        value_part = jnp.dot(columns, pieces[1], preferred_element_type=jnp.float32)
        return (totals[0] + gate_part, totals[1] + value_part)

    gate_sum, value_sum = over_all((gate_piece, value_piece), "fs", 0, add_rows, (empty, empty))
    down_block = lax.all_gather(down_piece, "fs", axis=1, tiled=True)
    hidden = (jax.nn.silu(gate_sum) * value_sum).astype(jnp.bfloat16)

    def row_term(start, count):
        rows = lax.dynamic_slice_in_dim(hidden, start, count, 0)
        return jnp.dot(rows, down_block, preferred_element_type=jnp.float32)

    return own_rows(row_term, normed.shape[0], "tp")


def on_device(
    tokens,
    mixer_output,
    early_norm,
    early_gate,
    early_value,
    early_down,
    early_post,
    mixer_gain,
    later_norm,
    later_gate,
    later_value,
    later_down,
    later_post,
):
    early_in = rms_scale(tokens, early_norm).astype(jnp.bfloat16)
    early_branch = half_branch(early_in, early_gate, early_value, early_down)
    mixed = (
        tokens.astype(jnp.float32)
        + 0.5 * rms_scale(early_branch, early_post)
        + rms_scale(mixer_output, mixer_gain)
    )
    mixed = mixed.astype(jnp.bfloat16)
    later_in = rms_scale(mixed, later_norm).astype(jnp.bfloat16)
    later_branch = half_branch(later_in, later_gate, later_value, later_down)
    layer_out = mixed.astype(jnp.float32) + 0.5 * rms_scale(later_branch, later_post)
    return layer_out.astype(jnp.bfloat16)


def solution(mesh):
    placed = (
        P(("rep", "fs", "tp"), None),
        P(("rep", "fs", "tp"), None),
        P(),
        P("fs", "tp"),
        P("fs", "tp"),
        P("tp", "fs"),
        P(),
        P(),
        P(),
        P("fs", "tp"),
        P("fs", "tp"),
        P("tp", "fs"),
        P(),
    )
    return jax.shard_map(
        on_device,
        mesh=mesh,
        in_specs=placed,
        out_specs=P(("rep", "fs", "tp"), None),
        check_vma=False,
    )
```

profile of v0, /device:TPU:1, one launch (start us, length us, event | category | flops | bytes accessed | tf_op | source)
XLA Modules:
  0.0 438.2 jit_solution(11551723246681318497)
XLA Ops:
  6.5 0.0 all-gather.9.cloned.1.call-start
  6.5 1.2 fusion.12
  7.8 2.0 fusion.14
  9.8 0.0 all-gather.9.cloned.1.call-update
  9.8 0.0 all-gather.11.cloned.1.call-start
  9.9 0.7 all-gather.11.cloned.1.call-update
  10.6 0.0 all-gather.13.cloned.1.call-start
  10.6 0.7 all-gather.13.cloned.1.call-update
  11.3 0.0 all-gather.15.cloned.1.call-start
  11.4 0.5 all-gather.15.cloned.1.call-update
  11.9 0.0 reduce-scatter.3.cloned.1.call-start
  11.9 32.1 %all-gather.9.cloned.1.call-done = bf16[512,2048]{1,0:T(8,128)(2,1)} async-done(((bf16[128,2048]{1,0:T(8,128)(2,1)}), bf16[512,2048]{1,0:T(8,128)(2,1)}) %all-gather.9.cloned.1.call-update) | async-done | bytes 2097168 | tf_op jit(solution)/shard_map/all_gather | solution.py:30
  44.0 41.1 %all-gather.11.cloned.1.call-done = bf16[2048,1280]{1,0:T(8,128)(2,1)} async-done(((bf16[128,1280]{1,0:T(8,128)(2,1)}), bf16[2048,1280]{1,0:T(8,128)(2,1)}) %all-gather.11.cloned.1.call-update) | async-done | bytes 5242896 | tf_op jit(solution)/shard_map/all_gather | solution.py:12
  85.1 7.5 %fusion.22 = f32[512,1280]{1,0:T(8,128)} fusion(bf16[512,2048]{1,0:T(8,128)(2,1)} %all-gather.9.cloned.1.call-done, bf16[2048,1280]{1,0:T(8,128)(2,1)} %all-gather.11.cloned.1.call-done), kind=kOutput, calls=%fused_computation.42 | convolution fusion | flops 2684354560 | bytes 9961472 | tf_op jit(solution)/shard_map/dot_general | solution.py:35
  92.6 33.7 %all-gather.13.cloned.1.call-done = bf16[2048,1280]{1,0:T(8,128)(2,1)} async-done(((bf16[128,1280]{1,0:T(8,128)(2,1)}), bf16[2048,1280]{1,0:T(8,128)(2,1)}) %all-gather.13.cloned.1.call-update) | async-done | bytes 5242896 | tf_op jit(solution)/shard_map/all_gather | solution.py:12
  126.3 51.5 %all-gather.15.cloned.1.call-done = bf16[1280,2048]{1,0:T(8,128)(2,1)} async-done(((bf16[1280,128]{1,0:T(8,128)(2,1)}), bf16[1280,2048]{1,0:T(8,128)(2,1)}) %all-gather.15.cloned.1.call-update) | async-done | bytes 5242896 | tf_op jit(solution)/shard_map/all_gather | solution.py:40
  177.8 0.0 copy-done.6
  177.8 12.5 %convolution_convert_fusion.1 = bf16[512,2048]{1,0:T(8,128)(2,1)} fusion(bf16[1280,2048]{1,0:T(8,128)(2,1)} %all-gather.15.cloned.1.call-done, bf16[512,2048]{1,0:T(8,128)(2,1)S(1)} %copy-done.6, bf16[2048,1280]{1,0:T(8,128)(2,1)} %all-gather.13.cloned.1.call-done, f32[512,1280]{1,0:T(8,128)} %fusion.22), kind=kOutput, calls=%fused_computation.5 | convolution fusion | flops 5373689856 | bytes 17301504 | tf_op jit(solution)/shard_map/dot_general | solution.py:45
  190.3 0.0 copy-start.4
  190.3 0.0 reduce-scatter.3.cloned.1.call-update
  190.3 0.0 all-gather.19.cloned.1.call-start
  190.4 0.5 all-gather.19.cloned.1.call-update
  190.9 0.0 all-gather.17.cloned.1.call-start
  190.9 0.4 copy-done.1
  191.3 0.2 fusion.5
  191.5 28.4 %reduce-scatter.3.cloned.1.call-done = bf16[128,2048]{1,0:T(8,128)(2,1)} async-done(((bf16[512,2048]{1,0:T(8,128)(2,1)}), bf16[128,2048]{1,0:T(8,128)(2,1)}) %reduce-scatter.3.cloned.1.call-update) | async-done | bytes 524304 | tf_op jit(solution)/shard_map/reduce_scatter | solution.py:19
  219.9 1.2 fusion.2
  221.2 0.0 copy-done
  221.2 0.0 copy-done.2
  221.2 1.6 fusion.15
  222.8 0.0 copy-done.4
  222.8 1.0 fusion.17
  223.8 0.0 all-gather.17.cloned.1.call-update
  223.8 0.0 all-gather.21.cloned.1.call-start
  223.9 0.7 all-gather.21.cloned.1.call-update
  224.6 0.0 all-gather.23.cloned.1.call-start
  224.6 0.7 all-gather.23.cloned.1.call-update
  225.3 0.2 reduce-scatter.5.cloned.1.call-start
  225.6 34.9 %all-gather.19.cloned.1.call-done = bf16[2048,1280]{1,0:T(8,128)(2,1)} async-done(((bf16[128,1280]{1,0:T(8,128)(2,1)}), bf16[2048,1280]{1,0:T(8,128)(2,1)}) %all-gather.19.cloned.1.call-update) | async-done | bytes 5242896 | tf_op jit(solution)/shard_map/all_gather | solution.py:12
  260.5 32.6 %all-gather.17.cloned.1.call-done = bf16[512,2048]{1,0:T(8,128)(2,1)} async-done(((bf16[128,2048]{1,0:T(8,128)(2,1)}), bf16[512,2048]{1,0:T(8,128)(2,1)}) %all-gather.17.cloned.1.call-update) | async-done | bytes 2097168 | tf_op jit(solution)/shard_map/all_gather | solution.py:30
  293.1 7.6 %fusion.23 = f32[512,1280]{1,0:T(8,128)} fusion(bf16[512,2048]{1,0:T(8,128)(2,1)} %all-gather.17.cloned.1.call-done, bf16[2048,1280]{1,0:T(8,128)(2,1)} %all-gather.19.cloned.1.call-done), kind=kOutput, calls=%fused_computation.43 | convolution fusion | flops 2684354560 | bytes 9961472 | tf_op jit(solution)/shard_map/dot_general | solution.py:35
  300.8 33.5 %all-gather.21.cloned.1.call-done = bf16[2048,1280]{1,0:T(8,128)(2,1)} async-done(((bf16[128,1280]{1,0:T(8,128)(2,1)}), bf16[2048,1280]{1,0:T(8,128)(2,1)}) %all-gather.21.cloned.1.call-update) | async-done | bytes 5242896 | tf_op jit(solution)/shard_map/all_gather | solution.py:12
  334.2 51.6 %all-gather.23.cloned.1.call-done = bf16[1280,2048]{1,0:T(8,128)(2,1)} async-done(((bf16[1280,128]{1,0:T(8,128)(2,1)}), bf16[1280,2048]{1,0:T(8,128)(2,1)}) %all-gather.23.cloned.1.call-update) | async-done | bytes 5242896 | tf_op jit(solution)/shard_map/all_gather | solution.py:40
  385.9 12.5 %convolution_convert_fusion = bf16[512,2048]{1,0:T(8,128)(2,1)} fusion(bf16[1280,2048]{1,0:T(8,128)(2,1)} %all-gather.23.cloned.1.call-done, bf16[512,2048]{1,0:T(8,128)(2,1)S(1)} %copy-done.7, bf16[2048,1280]{1,0:T(8,128)(2,1)} %all-gather.21.cloned.1.call-done, f32[512,1280]{1,0:T(8,128)} %fusion.23), kind=kOutput, calls=%fused_computation.4 | convolution fusion | flops 5373689856 | bytes 17301504 | tf_op jit(solution)/shard_map/dot_general | solution.py:45
  398.4 0.0 reduce-scatter.5.cloned.1.call-update
  398.4 29.6 %reduce-scatter.5.cloned.1.call-done = bf16[128,2048]{1,0:T(8,128)(2,1)} async-done(((bf16[512,2048]{1,0:T(8,128)(2,1)}), bf16[128,2048]{1,0:T(8,128)(2,1)}) %reduce-scatter.5.cloned.1.call-update) | async-done | bytes 524304 | tf_op jit(solution)/shard_map/reduce_scatter | solution.py:19
  428.0 1.2 fusion.9
  429.2 2.1 fusion.18
  (15 shorter events, 0.1 us)
Async XLA Ops:
  6.5 37.5 %all-gather.9.cloned.1.call-start = ((), (), s32[]{:S(2)}) async-start(), calls=%async_computation.2 | async-start | bytes 2621440 | tf_op jit(solution)/shard_map/all_gather | solution.py:30
  9.8 75.3 %all-gather.11.cloned.1.call-start = ((), (), s32[]{:S(2)}) async-start(), calls=%async_computation.3 | async-start | bytes 5570560 | tf_op jit(solution)/shard_map/all_gather | solution.py:12
  10.6 115.7 %all-gather.13.cloned.1.call-start = ((), (), s32[]{:S(2)}) async-start(), calls=%async_computation.4 | async-start | bytes 5570560 | tf_op jit(solution)/shard_map/all_gather | solution.py:12
  11.3 166.5 %all-gather.15.cloned.1.call-start = ((), (), s32[]{:S(2)}) async-start(), calls=%async_computation.5 | async-start | bytes 5570560 | tf_op jit(solution)/shard_map/all_gather | solution.py:40
  11.9 208.0 %reduce-scatter.3.cloned.1.call-start = ((), (), s32[]{:S(2)}) async-start(), calls=%async_computation.6 | async-start | bytes 2621440 | tf_op jit(solution)/shard_map/reduce_scatter | solution.py:19
  44.0 133.8 %copy-start.6 = (bf16[512,2048]{1,0:T(8,128)(2,1)S(1)}, bf16[512,2048]{1,0:T(8,128)(2,1)}, u32[]{:S(2)}) copy-start(bf16[512,2048]{1,0:T(8,128)(2,1)} %all-gather.9.cloned.1.call-done) | copy-start | bytes 6291460
  190.3 1.0 copy-start.1
  190.3 30.9 %copy-start = (bf16[128,2048]{1,0:T(8,128)(2,1)S(1)}, bf16[128,2048]{1,0:T(8,128)(2,1)}, u32[]{:S(2)}) copy-start(bf16[128,2048]{1,0:T(8,128)(2,1)} %param.13) | copy-start | bytes 1572868
  190.3 30.9 %copy-start.2 = (f32[2048]{0:T(1024)S(1)}, f32[2048]{0:T(1024)}, u32[]{:S(2)}) copy-start(f32[2048]{0:T(1024)} %param.20) | copy-start | bytes 24580
  190.3 30.9 %copy-start.3 = (f32[2048]{0:T(1024)S(1)}, f32[2048]{0:T(1024)}, u32[]{:S(2)}) copy-start(f32[2048]{0:T(1024)} %param.19) | copy-start | bytes 24580
  190.3 32.6 %copy-start.4 = (f32[2048]{0:T(1024)S(1)}, f32[2048]{0:T(1024)}, u32[]{:S(2)}) copy-start(f32[2048]{0:T(1024)} %param.21) | copy-start | bytes 24580
  190.3 70.2 %all-gather.19.cloned.1.call-start = ((), (), s32[]{:S(2)}) async-start(), calls=%async_computation.8 | async-start | bytes 5570560 | tf_op jit(solution)/shard_map/all_gather | solution.py:12
  190.9 102.2 %all-gather.17.cloned.1.call-start = ((), (), s32[]{:S(2)}) async-start(), calls=%async_computation.7 | async-start | bytes 2621440 | tf_op jit(solution)/shard_map/all_gather | solution.py:30
  223.8 110.4 %all-gather.21.cloned.1.call-start = ((), (), s32[]{:S(2)}) async-start(), calls=%async_computation.9 | async-start | bytes 5570560 | tf_op jit(solution)/shard_map/all_gather | solution.py:12
  224.6 161.2 %all-gather.23.cloned.1.call-start = ((), (), s32[]{:S(2)}) async-start(), calls=%async_computation.10 | async-start | bytes 5570560 | tf_op jit(solution)/shard_map/all_gather | solution.py:40
  225.3 202.7 %reduce-scatter.5.cloned.1.call-start = ((), (), s32[]{:S(2)}) async-start(), calls=%async_computation.11 | async-start | bytes 2621440 | tf_op jit(solution)/shard_map/reduce_scatter | solution.py:19
  293.1 92.7 %copy-start.7 = (bf16[512,2048]{1,0:T(8,128)(2,1)S(1)}, bf16[512,2048]{1,0:T(8,128)(2,1)}, u32[]{:S(2)}) copy-start(bf16[512,2048]{1,0:T(8,128)(2,1)} %all-gather.17.cloned.1.call-done) | copy-start | bytes 6291460
  398.3 30.9 %copy-start.5 = (f32[2048]{0:T(1024)S(1)}, f32[2048]{0:T(1024)}, u32[]{:S(2)}) copy-start(f32[2048]{0:T(1024)} %param.25) | copy-start | bytes 24580
Sparse Core Ops, SparseCore 0:
  9.9 34.0 all-gather.8
  45.7 39.3 all-gather.10
  86.8 39.4 all-gather.12
  127.8 49.9 all-gather.14
  190.4 29.4 reduce-scatter.2
  221.5 38.9 all-gather.18
  262.2 30.9 all-gather.16
  294.8 39.3 all-gather.20
  335.9 49.9 all-gather.22
  398.5 29.4 reduce-scatter.4
where the time goes:
time: 439 us; the launch traced here: 438 us
  waiting for transfers between devices  373 us (85%)
  matrix products  40.1 us (9%)
  between operations  13.6 us (3%)
  other arithmetic  10.7 us (2%)
    all_gather x4, waiting for transfers between devices, gathered(): return lax.all_gather(part, axis, axis=dim, tiled=True)  143 us
    all_gather x2, waiting for transfers between devices, half_branch(): down_block = lax.all_gather(down_piece, 'fs', axis=1, tiled=True)  103 us
    all_gather x2, waiting for transfers between devices, half_branch(): all_rows = lax.all_gather(normed, 'tp', axis=0, tiled=True)  64.7 us
    reduce_scatter x2, waiting for transfers between devices, own_rows(): lax.psum_scatter(everything.astype(jnp.bfloat16), axis, scatter_dimension...  58.1 us
    dot_general x2, matrix products, row_term(): return jnp.dot(rows, down_block, preferred_element_type=jnp.float32)  25 us
    dot_general x2, matrix products, add_rows(): gate_part = jnp.dot(columns, pieces[0], preferred_element_type=jnp.float32)  15.1 us
  transfers between devices with their start and end apart: 10, of which 10 were waited for; matrix products, arithmetic and copies ran while one was open for 4% of the time, Pallas kernels for 0%

commit v1 on v0

--- a/solution.py
+++ b/solution.py
@@ -4,6 +4,27 @@
 from jax.sharding import PartitionSpec as P
 
 epsilon = 1e-06
+
+
+def _advance_block(point, along_dim):
+    moved = list(point.shape[1:])
+    moved[along_dim] *= point.shape[0]
+    s_next = jnp.moveaxis(point, 0, along_dim).reshape(moved)
+    return s_next
+
+
+def process_the_corner(local_block, which_axis):
+    now = local_block[None]
+    how_many = jax.lax.psum(1, axis_name=which_axis)
+    for i0 in range(how_many.bit_length() - 1):
+        known = 1 << i0
+        z2 = jax.lax.ppermute(
+            now, axis_name=which_axis, perm=[(k0, k0 ^ known) for k0 in range(how_many)]
+        )
+        y = jnp.stack([now, z2], 0)
+        b_next = jax.lax.axis_index(which_axis) >> i0 & 1
+        now = jnp.where(b_next == 0, y, y[::-1]).reshape(-1, *local_block.shape)
+    return now
 
 
 def over_all(piece, axis, dim, step, start):
@@ -27,7 +48,12 @@
 
 
 def half_branch(normed, gate_piece, value_piece, down_piece):
-    all_rows = lax.all_gather(normed, "tp", axis=0, tiled=True)
+
+    def _cover_loads(work_x, block_in, array_dim=0):
+        seen_now = _advance_block(process_the_corner(work_x, block_in), array_dim)
+        return seen_now
+
+    all_rows = _cover_loads(normed, "tp")
     empty = jnp.zeros((all_rows.shape[0], gate_piece.shape[1]), jnp.float32)
 
     def add_rows(totals, pieces, start):

time: 439 us -> 373 us (0.85)
  waiting for transfers between devices: 373 us -> 301 us
  starting transfers between devices: 0.54 us -> 7.53 us
    ppermute x0 -> x4, waiting for transfers between devices: none -> 70.3 us  [process_the_corner(): jax.lax.ppermute(now, axis_name=which_axis, perm=[(k0, k0 ^ known) for k0...]
    all_gather x4, waiting for transfers between devices: 143 us -> 73.4 us  [gathered(): return lax.all_gather(part, axis, axis=dim, tiled=True)]
    all_gather x2 -> x0, waiting for transfers between devices: 64.7 us -> none  [half_branch(): all_rows = lax.all_gather(normed, 'tp', axis=0, tiled=True)]
    ppermute x0 -> x4, starting transfers between devices: none -> 7.26 us  [process_the_corner(): jax.lax.ppermute(now, axis_name=which_axis, perm=[(k0, k0 ^ known) for k0...]
    all_gather x2, waiting for transfers between devices: 103 us -> 95.8 us  [half_branch(): down_block = lax.all_gather(down_piece, 'fs', axis=1, tiled=True)]
  transfers between devices with their start and end apart: 10 -> 12, of which waited for: 10 -> 10; matrix products, arithmetic and copies ran while one was open for 4% -> 6% of each run, Pallas kernels for 0% -> 0%
where the time goes in v1:
time: 373 us; the launch traced here: 372 us
  waiting for transfers between devices  301 us (81%)
  matrix products  38.7 us (10%)
  between operations  13.6 us (4%)
  other arithmetic  11.2 us (3%)
  starting transfers between devices  7.53 us (2%)
    all_gather x2, waiting for transfers between devices, half_branch(): down_block = lax.all_gather(down_piece, 'fs', axis=1, tiled=True)  95.8 us
    all_gather x4, waiting for transfers between devices, gathered(): return lax.all_gather(part, axis, axis=dim, tiled=True)  73.4 us
    ppermute x4, waiting for transfers between devices, process_the_corner(): jax.lax.ppermute(now, axis_name=which_axis, perm=[(k0, k0 ^ known) for k0...  70.3 us
    reduce_scatter x2, waiting for transfers between devices, own_rows(): lax.psum_scatter(everything.astype(jnp.bfloat16), axis, scatter_dimension...  57.6 us
    dot_general x2, matrix products, row_term(): return jnp.dot(rows, down_block, preferred_element_type=jnp.float32)  25 us
    dot_general x2, matrix products, add_rows(): gate_part = jnp.dot(columns, pieces[0], preferred_element_type=jnp.float32)  13.7 us
  transfers between devices with their start and end apart: 12, of which 10 were waited for; matrix products, arithmetic and copies ran while one was open for 6% of the time, Pallas kernels for 0%

profile of v1, /device:TPU:1, one launch (start us, length us, event | category | flops | bytes accessed | tf_op | source)
XLA Modules:
  0.0 372.1 jit_solution(9268040958646858422)
XLA Ops:
  6.5 0.7 all-gather.7.cloned.1.call-update
  7.3 0.0 all-gather.11.cloned.1.call-start
  7.3 0.7 all-gather.11.cloned.1.call-update
  8.0 0.0 all-gather.9.cloned.1.call-start
  8.1 0.7 all-gather.9.cloned.1.call-update
  8.7 0.0 reduce-scatter.3.cloned.1.call-start
  8.8 1.2 fusion.12
  10.0 1.3 fusion.26
  11.3 2.5 collective-permute-start
  13.8 11.7 %collective-permute-done = bf16[1,128,2048]{2,1,0:T(8,128)(2,1)S(1)} collective-permute-done((bf16[1,128,2048]{2,1,0:T(8,128)(2,1)S(1)}, bf16[1,128,2048]{2,1,0:T(8,128)(2,1)S(1)}, u32[]{:S(2)}, u32[]{:S(2)}) %collective-permute-start) | collective-permute-done | bytes 524320 | tf_op jit(solution)/shard_map/ppermute | solution.py:21
  25.5 0.1 pad_maximum_fusion.2
  25.7 0.4 fusion.20
  26.1 3.2 collective-permute-start.1
  29.3 22.1 %collective-permute-done.1 = bf16[2,128,2048]{2,1,0:T(8,128)(2,1)S(1)} collective-permute-done((bf16[2,128,2048]{2,1,0:T(8,128)(2,1)S(1)}, bf16[2,128,2048]{2,1,0:T(8,128)(2,1)S(1)}, u32[]{:S(2)}, u32[]{:S(2)}) %collective-permute-start.1) | collective-permute-done | bytes 1048608 | tf_op jit(solution)/shard_map/ppermute | solution.py:21
  51.4 0.2 pad_maximum_fusion
  51.6 0.5 reverse_select_fusion.1
  52.1 0.0 all-gather.7.cloned.1.call-done
  52.1 6.9 %fusion.30 = f32[512,1280]{1,0:T(8,128)} fusion(bf16[512,2048]{1,0:T(8,128)(2,1)S(1)} %bitcast.42, bf16[2048,1280]{1,0:T(8,128)(2,1)} %all-gather.7.cloned.1.call-done), kind=kOutput, calls=%fused_computation.58 | convolution fusion | flops 2684354560 | bytes 9961472 | tf_op jit(solution)/shard_map/dot_general | solution.py:61
  59.0 44.2 %all-gather.11.cloned.1.call-done = bf16[1280,2048]{1,0:T(8,128)(2,1)} async-done(((bf16[1280,128]{1,0:T(8,128)(2,1)}), bf16[1280,2048]{1,0:T(8,128)(2,1)}) %all-gather.11.cloned.1.call-update) | async-done | bytes 5242896 | tf_op jit(solution)/shard_map/all_gather | solution.py:66
  103.2 40.7 %all-gather.9.cloned.1.call-done = bf16[2048,1280]{1,0:T(8,128)(2,1)} async-done(((bf16[128,1280]{1,0:T(8,128)(2,1)}), bf16[2048,1280]{1,0:T(8,128)(2,1)}) %all-gather.9.cloned.1.call-update) | async-done | bytes 5242896 | tf_op jit(solution)/shard_map/all_gather | solution.py:33
  143.9 12.5 %convolution_convert_fusion.1 = bf16[512,2048]{1,0:T(8,128)(2,1)} fusion(bf16[1280,2048]{1,0:T(8,128)(2,1)} %all-gather.11.cloned.1.call-done, bf16[512,2048]{1,0:T(8,128)(2,1)S(1)} %bitcast.43, bf16[2048,1280]{1,0:T(8,128)(2,1)} %all-gather.9.cloned.1.call-done, f32[512,1280]{1,0:T(8,128)} %fusion.30), kind=kOutput, calls=%fused_computation.7 | convolution fusion | flops 5373689856 | bytes 17301504 | tf_op jit(solution)/shard_map/dot_general | solution.py:71
  156.4 0.0 all-gather.13.cloned.1.call-start
  156.5 0.5 all-gather.13.cloned.1.call-update
  157.0 0.0 all-gather.15.cloned.1.call-start
  157.0 0.5 all-gather.15.cloned.1.call-update
  157.6 0.0 all-gather.17.cloned.1.call-start
  157.6 0.7 all-gather.17.cloned.1.call-update
  158.3 0.0 reduce-scatter.5.cloned.1.call-start
  158.4 0.2 fusion.5
  158.6 28.0 %reduce-scatter.3.cloned.1.call-done = bf16[128,2048]{1,0:T(8,128)(2,1)} async-done(((bf16[512,2048]{1,0:T(8,128)(2,1)}), bf16[128,2048]{1,0:T(8,128)(2,1)}) %reduce-scatter.3.cloned.1.call-update) | async-done | bytes 524304 | tf_op jit(solution)/shard_map/reduce_scatter | solution.py:40
  186.6 1.2 fusion.2
  187.8 1.6 fusion.15
  189.5 0.2 fusion.24
  189.7 0.1 collective-permute-start.2
  189.8 12.8 %collective-permute-done.2 = bf16[1,128,2048]{2,1,0:T(8,128)(2,1)S(1)} collective-permute-done((bf16[1,128,2048]{2,1,0:T(8,128)(2,1)S(1)}, bf16[1,128,2048]{2,1,0:T(8,128)(2,1)S(1)}, u32[]{:S(2)}, u32[]{:S(2)}) %collective-permute-start.2) | collective-permute-done | bytes 524320 | tf_op jit(solution)/shard_map/ppermute | solution.py:21
  202.6 0.1 pad_maximum_fusion.3
  202.7 0.2 fusion.22
  202.9 1.4 collective-permute-start.3
  204.3 23.6 %collective-permute-done.3 = bf16[2,128,2048]{2,1,0:T(8,128)(2,1)S(1)} collective-permute-done((bf16[2,128,2048]{2,1,0:T(8,128)(2,1)S(1)}, bf16[2,128,2048]{2,1,0:T(8,128)(2,1)S(1)}, u32[]{:S(2)}, u32[]{:S(2)}) %collective-permute-start.3) | collective-permute-done | bytes 1048608 | tf_op jit(solution)/shard_map/ppermute | solution.py:21
  227.9 0.2 pad_maximum_fusion.1
  228.1 0.5 reverse_select_fusion
  228.6 6.9 %fusion.31 = f32[512,1280]{1,0:T(8,128)} fusion(bf16[512,2048]{1,0:T(8,128)(2,1)S(1)} %bitcast.40, bf16[2048,1280]{1,0:T(8,128)(2,1)} %all-gather.13.cloned.1.call-done), kind=kOutput, calls=%fused_computation.59 | convolution fusion | flops 2684354560 | bytes 9961472 | tf_op jit(solution)/shard_map/dot_general | solution.py:61
  235.5 32.7 %all-gather.15.cloned.1.call-done = bf16[2048,1280]{1,0:T(8,128)(2,1)} async-done(((bf16[128,1280]{1,0:T(8,128)(2,1)}), bf16[2048,1280]{1,0:T(8,128)(2,1)}) %all-gather.15.cloned.1.call-update) | async-done | bytes 5242896 | tf_op jit(solution)/shard_map/all_gather | solution.py:33
  268.2 51.6 %all-gather.17.cloned.1.call-done = bf16[1280,2048]{1,0:T(8,128)(2,1)} async-done(((bf16[1280,128]{1,0:T(8,128)(2,1)}), bf16[1280,2048]{1,0:T(8,128)(2,1)}) %all-gather.17.cloned.1.call-update) | async-done | bytes 5242896 | tf_op jit(solution)/shard_map/all_gather | solution.py:66
  319.8 12.5 %convolution_convert_fusion = bf16[512,2048]{1,0:T(8,128)(2,1)} fusion(bf16[1280,2048]{1,0:T(8,128)(2,1)} %all-gather.17.cloned.1.call-done, bf16[512,2048]{1,0:T(8,128)(2,1)S(1)} %bitcast.41, bf16[2048,1280]{1,0:T(8,128)(2,1)} %all-gather.15.cloned.1.call-done, f32[512,1280]{1,0:T(8,128)} %fusion.31), kind=kOutput, calls=%fused_computation.6 | convolution fusion | flops 5373689856 | bytes 17301504 | tf_op jit(solution)/shard_map/dot_general | solution.py:71
  332.3 29.6 %reduce-scatter.5.cloned.1.call-done = bf16[128,2048]{1,0:T(8,128)(2,1)} async-done(((bf16[512,2048]{1,0:T(8,128)(2,1)}), bf16[128,2048]{1,0:T(8,128)(2,1)}) %reduce-scatter.5.cloned.1.call-update) | async-done | bytes 524304 | tf_op jit(solution)/shard_map/reduce_scatter | solution.py:40
  361.9 1.2 fusion.9
  363.1 2.1 fusion.18
  (21 shorter events, 0.1 us)
Async XLA Ops:
  6.5 45.6 %all-gather.7.cloned.1.call-start = ((), (), s32[]{:S(2)}) async-start(), calls=%async_computation.2 | async-start | bytes 5570560 | tf_op jit(solution)/shard_map/all_gather | solution.py:33
  7.3 95.9 %all-gather.11.cloned.1.call-start = ((), (), s32[]{:S(2)}) async-start(), calls=%async_computation.4 | async-start | bytes 5570560 | tf_op jit(solution)/shard_map/all_gather | solution.py:66
  8.0 135.9 %all-gather.9.cloned.1.call-start = ((), (), s32[]{:S(2)}) async-start(), calls=%async_computation.3 | async-start | bytes 5570560 | tf_op jit(solution)/shard_map/all_gather | solution.py:33
  8.7 177.8 %reduce-scatter.3.cloned.1.call-start = ((), (), s32[]{:S(2)}) async-start(), calls=%async_computation.5 | async-start | bytes 2621440 | tf_op jit(solution)/shard_map/reduce_scatter | solution.py:40
  11.3 14.3 %collective-permute-start = (bf16[1,128,2048]{2,1,0:T(8,128)(2,1)S(1)}, bf16[1,128,2048]{2,1,0:T(8,128)(2,1)S(1)}, u32[]{:S(2)}, u32[]{:S(2)}) collective-permute-start(bf16[1,128,2048]{2,1,0:T(8,128)(2,1)S(1)} %get-tuple-element.14), channel_id=1, source_target_pairs={{0,1},{1,0},{2,3},{3,2},{4,5},{5,4},{6,7},{7,6},{8,9},{9,8},{10,11... | collective-permute-start | bytes 1572872 | tf_op jit(solution)/shard_map/ppermute | solution.py:21
  26.1 25.3 %collective-permute-start.1 = (bf16[2,128,2048]{2,1,0:T(8,128)(2,1)S(1)}, bf16[2,128,2048]{2,1,0:T(8,128)(2,1)S(1)}, u32[]{:S(2)}, u32[]{:S(2)}) collective-permute-start(bf16[2,128,2048]{2,1,0:T(8,128)(2,1)S(1)} %get-tuple-element.10), channel_id=1, source_target_pairs={{0,2},{1,3},{2,0},{3,1},{4,6},{5,7},{6,4},{7,5},{8,10},{9,11},{10,... | collective-permute-start | bytes 3145736 | tf_op jit(solution)/shard_map/ppermute | solution.py:21
  156.4 2.0 copy-start.1
  156.4 31.4 %copy-start = (bf16[128,2048]{1,0:T(8,128)(2,1)S(1)}, bf16[128,2048]{1,0:T(8,128)(2,1)}, u32[]{:S(2)}) copy-start(bf16[128,2048]{1,0:T(8,128)(2,1)} %param.13) | copy-start | bytes 1572868
  156.4 31.4 %copy-start.2 = (f32[2048]{0:T(1024)S(1)}, f32[2048]{0:T(1024)}, u32[]{:S(2)}) copy-start(f32[2048]{0:T(1024)} %param.20) | copy-start | bytes 24580
  156.4 31.5 %copy-start.3 = (f32[2048]{0:T(1024)S(1)}, f32[2048]{0:T(1024)}, u32[]{:S(2)}) copy-start(f32[2048]{0:T(1024)} %param.19) | copy-start | bytes 24580
  156.4 33.1 %copy-start.4 = (f32[2048]{0:T(1024)S(1)}, f32[2048]{0:T(1024)}, u32[]{:S(2)}) copy-start(f32[2048]{0:T(1024)} %param.21) | copy-start | bytes 24580
  156.4 72.2 %all-gather.13.cloned.1.call-start = ((), (), s32[]{:S(2)}) async-start(), calls=%async_computation.6 | async-start | bytes 5570560 | tf_op jit(solution)/shard_map/all_gather | solution.py:33
  157.0 111.2 %all-gather.15.cloned.1.call-start = ((), (), s32[]{:S(2)}) async-start(), calls=%async_computation.7 | async-start | bytes 5570560 | tf_op jit(solution)/shard_map/all_gather | solution.py:33
  157.6 162.2 %all-gather.17.cloned.1.call-start = ((), (), s32[]{:S(2)}) async-start(), calls=%async_computation.8 | async-start | bytes 5570560 | tf_op jit(solution)/shard_map/all_gather | solution.py:66
  158.3 203.6 %reduce-scatter.5.cloned.1.call-start = ((), (), s32[]{:S(2)}) async-start(), calls=%async_computation.9 | async-start | bytes 2621440 | tf_op jit(solution)/shard_map/reduce_scatter | solution.py:40
  189.7 12.9 %collective-permute-start.2 = (bf16[1,128,2048]{2,1,0:T(8,128)(2,1)S(1)}, bf16[1,128,2048]{2,1,0:T(8,128)(2,1)S(1)}, u32[]{:S(2)}, u32[]{:S(2)}) collective-permute-start(bf16[1,128,2048]{2,1,0:T(8,128)(2,1)S(1)} %get-tuple-element.12), channel_id=1, source_target_pairs={{0,1},{1,0},{2,3},{3,2},{4,5},{5,4},{6,7},{7,6},{8,9},{9,8},{10,11... | collective-permute-start | bytes 1572872 | tf_op jit(solution)/shard_map/ppermute | solution.py:21
  202.9 25.0 %collective-permute-start.3 = (bf16[2,128,2048]{2,1,0:T(8,128)(2,1)S(1)}, bf16[2,128,2048]{2,1,0:T(8,128)(2,1)S(1)}, u32[]{:S(2)}, u32[]{:S(2)}) collective-permute-start(bf16[2,128,2048]{2,1,0:T(8,128)(2,1)S(1)} %get-tuple-element.8), channel_id=1, source_target_pairs={{0,2},{1,3},{2,0},{3,1},{4,6},{5,7},{6,4},{7,5},{8,10},{9,11},{10,... | collective-permute-start | bytes 3145736 | tf_op jit(solution)/shard_map/ppermute | solution.py:21
  332.2 30.9 %copy-start.5 = (f32[2048]{0:T(1024)S(1)}, f32[2048]{0:T(1024)}, u32[]{:S(2)}) copy-start(f32[2048]{0:T(1024)} %param.25) | copy-start | bytes 24580
Sparse Core Ops, SparseCore 0:
  9.0 42.5 all-gather.6
  53.2 49.9 all-gather.10
  104.9 38.9 all-gather.8
  156.5 29.9 reduce-scatter.2
  188.1 39.1 all-gather.12
  228.9 39.2 all-gather.14
  269.8 49.9 all-gather.16
  332.4 29.4 reduce-scatter.4
